TPU v7x, 32 devices: a whole 2x2x4 slice. The times are simulated.
32 devices in a mesh: sp: 16 (over z, y, x), tp: 2 (over core).
Axes of the slice: x: 2, y: 2, z: 4, core: 2. Of those that a mesh axis runs over, the one named last changes fastest.
Arguments:
- stream: bfloat16 [2048, 2048], P('sp', 'tp'), may hold values from -14 to 14
- queries: bfloat16 [2048, 2048], P('sp', 'tp'), may hold values from -6 to 6
- key_rows: bfloat16 [2048, 2048], P('sp', 'tp'), may hold values from -6 to 6
- values: bfloat16 [2048, 2048], P('sp', 'tp'), may hold values from -6 to 6
- out_gate: bfloat16 [2048, 2048], P('sp', 'tp'), may hold values from -6 to 6
- in_gate: float32 [16, 2048], P('tp', 'sp'), may hold values from -4 to 120
- forget_gate: float32 [16, 2048], P('tp', 'sp'), may hold values from -1 to 20
- head_gain: float32 [2048], P('tp'), may hold values from 0.1 to 1.9
- w_out: bfloat16 [2048, 2048], P('tp'), may hold values from -0.30935922 to 0.30935922
- norm_gains: bfloat16 [3, 2048], P(None, 'tp'), may hold values from 0.099609375 to 1.8984375
- w_gate: bfloat16 [2048, 5632], P('sp', 'tp'), may hold values from -0.125 to 0.125
- w_up: bfloat16 [2048, 5632], P('sp', 'tp'), may hold values from -0.125 to 0.125
- w_down: bfloat16 [5632, 2048], P('tp', 'sp'), may hold values from -0.18655063 to 0.18655063
Outputs:
- result: bfloat16 [2048, 2048], P('sp', 'tp')
All inputs are finite; a program needn't handle non-finite values.
Results may differ from a plain program's by a relative error of at most 0.012.
Values may be sent and summed in bfloat16 or wider, within the bound.
No kernel may reach another device: no remote copies, remote signals or barrier semaphores. Data moves between devices by JAX's collectives and lax.ppermute only.
A program may use at most 128 MiB of HBM per device.

v0:
```python
import jax
import jax.numpy as jnp
from jax import lax
from jax.sharding import PartitionSpec as P

D = 2048
BLOCK = 128
EPS = 1e-06


def carried_in(value, axis, combine, identity):
    peers, position = (lax.axis_size(axis), lax.axis_index(axis))
    everything = jax.tree.map(lambda part: lax.all_gather(part, axis), value)
    start = jax.tree.map(
        lambda part, zero: jnp.broadcast_to(jnp.asarray(zero, part.dtype), part.shape),
        value,
        identity,
    )

    def turn(k, before):
        reached = k < position
        new = combine(before, jax.tree.map(lambda part: part[k], everything))
        return jax.tree.map(lambda a, b: jnp.where(reached, a, b), new, before)

    return lax.fori_loop(0, peers, turn, start)


def join_states(earlier, later):
    total_early, summit_early, memory_early = earlier
    total_late, summit_late, memory_late = later
    summit = jnp.maximum(total_late + summit_early, summit_late)
    scale_early = jnp.exp(total_late + summit_early - summit)
    scale_late = jnp.exp(summit_late - summit)
    memory = scale_early[:, None, None] * memory_early + scale_late[:, None, None] * memory_late
    return (total_early + total_late, summit, memory)


def cell_block(queries, key_rows, values, in_gate, forget_gate):
    highest = lax.Precision.HIGHEST
    tokens_here = queries.shape[0]
    heads_here = in_gate.shape[0]
    head_dim = queries.shape[1] // heads_here
    blocks = tokens_here // BLOCK
    key_scale = head_dim ** (-0.5)
    log_forget = jax.nn.log_sigmoid(forget_gate)
    cumulative = jnp.cumsum(log_forget, axis=1)
    total_log = cumulative[:, -1]
    toward = total_log[:, None] - cumulative + in_gate
    summit = jnp.max(toward, axis=1)
    weight_key = jnp.exp(toward - summit[:, None])
    key_scaled = key_rows.astype(jnp.float32).reshape(tokens_here, heads_here, head_dim) * key_scale
    value_float = values.astype(jnp.float32).reshape(tokens_here, heads_here, head_dim)
    weighted = key_scaled * weight_key.T[:, :, None]
    memory_dev = jnp.einsum("shd,she->hde", weighted, value_float, precision=highest)
    identity = (jnp.zeros_like(total_log), jnp.full_like(summit, -1e30), jnp.zeros_like(memory_dev))
    prior_total, prior_summit, prior_memory = carried_in(
        (total_log, summit, memory_dev), "sp", join_states, identity
    )
    start_summit = jnp.maximum(prior_total, prior_summit)
    carry_scale = jnp.exp(prior_summit - start_summit)
    start_memory = carry_scale[:, None, None] * prior_memory
    query_blocks = queries.reshape(blocks, BLOCK, heads_here, head_dim)
    key_blocks = key_rows.reshape(blocks, BLOCK, heads_here, head_dim)
    value_blocks = values.reshape(blocks, BLOCK, heads_here, head_dim)
    keyf_blocks = key_scaled.reshape(blocks, BLOCK, heads_here, head_dim)
    forget_blocks = log_forget.reshape(heads_here, blocks, BLOCK).transpose(1, 0, 2)
    input_blocks = in_gate.reshape(heads_here, blocks, BLOCK).transpose(1, 0, 2)
    causal = jnp.tril(jnp.ones((BLOCK, BLOCK), dtype=bool))

    def advance(carried, inputs):
        memory, stabil = carried
        query_blk, key_blk, value_blk, keyf_blk, forget_blk, input_blk = inputs
        cumul_blk = jnp.cumsum(forget_blk, axis=-1)
        within = jnp.where(
            causal, cumul_blk[:, :, None] - cumul_blk[:, None, :] + input_blk[:, None, :], -jnp.inf
        )
        across = cumul_blk + stabil[:, None]
        stable = jnp.maximum(across, jnp.max(within, axis=-1))
        weight_in = jnp.exp(within - stable[:, :, None])
        weight_out = jnp.exp(across - stable)
        raw_scores = (
            jnp.einsum("thd,shd->hts", query_blk, key_blk, preferred_element_type=jnp.float32)
            * key_scale
        )
        scores = raw_scores * weight_in
        probs_low = scores.astype(jnp.bfloat16)
        query_float = query_blk.astype(jnp.float32)
        output = jnp.einsum(
            "hts,shd->htd", probs_low, value_blk, preferred_element_type=jnp.float32
        )
        output = output + weight_out[:, :, None] * jnp.einsum(
            "thd,hde->hte", query_float, memory, precision=highest
        )
        last_sum = cumul_blk[:, -1]
        toward_blk = last_sum[:, None] - cumul_blk + input_blk
        stabil_new = jnp.maximum(last_sum + stabil, jnp.max(toward_blk, axis=-1))
        decay_now = jnp.exp(last_sum + stabil - stabil_new)
        weight_blk = jnp.exp(toward_blk - stabil_new[:, None])
        weighted_blk = keyf_blk * weight_blk.T[:, :, None]
        memory_new = decay_now[:, None, None] * memory + jnp.einsum(
            "shd,she->hde", weighted_blk, value_blk.astype(jnp.float32), precision=highest
        )
        return ((memory_new, stabil_new), output.transpose(1, 0, 2))

    _, outputs = lax.scan(
        advance,
        (start_memory, start_summit),
        (query_blocks, key_blocks, value_blocks, keyf_blocks, forget_blocks, input_blocks),
    )
    return outputs.reshape(tokens_here, heads_here, head_dim)


def shards(
    stream,
    queries,
    key_rows,
    values,
    out_gate,
    in_gate,
    forget_gate,
    head_gain,
    w_out,
    norm_gains,
    w_gate,
    w_up,
    w_down,
):
    tokens_here = queries.shape[0]
    cell = cell_block(queries, key_rows, values, in_gate, forget_gate)
    normed_cell = cell * lax.rsqrt(jnp.mean(cell * cell, axis=-1, keepdims=True) + EPS)
    mixed = (
        normed_cell.reshape(tokens_here, -1)
        * head_gain
        * jax.nn.sigmoid(out_gate.astype(jnp.float32))
    ).astype(jnp.bfloat16)
    partial_mix = jnp.dot(mixed, w_out, preferred_element_type=jnp.float32)
    own_gains = norm_gains.astype(jnp.float32)
    mix_sum = lax.psum_scatter(
        partial_mix.astype(jnp.bfloat16), "tp", scatter_dimension=1, tiled=True
    ).astype(jnp.float32)
    mix_squares = lax.psum(jnp.sum(mix_sum * mix_sum, axis=1), "tp")
    mix_norm = mix_sum * lax.rsqrt(mix_squares / D + EPS)[:, None] * own_gains[0]
    after_mix = (stream.astype(jnp.float32) + mix_norm).astype(jnp.bfloat16)
    kept_rows = after_mix.astype(jnp.float32)
    resid_squares = lax.psum(jnp.sum(kept_rows * kept_rows, axis=1), "tp")
    normed = (kept_rows * lax.rsqrt(resid_squares / D + EPS)[:, None] * own_gains[1]).astype(
        jnp.bfloat16
    )
    normed_all = lax.all_gather(normed, "tp", axis=1, tiled=True)
    gate_part = jnp.dot(
        normed_all,
        lax.all_gather(w_gate, "sp", axis=0, tiled=True),
        preferred_element_type=jnp.float32,
    )
    up_part = jnp.dot(
        normed_all,
        lax.all_gather(w_up, "sp", axis=0, tiled=True),
        preferred_element_type=jnp.float32,
    )
    hidden = (jax.nn.silu(gate_part) * up_part).astype(jnp.bfloat16)
    ffn_terms = jnp.dot(
        hidden, lax.all_gather(w_down, "sp", axis=1, tiled=True), preferred_element_type=jnp.float32
    )
    ffn_sum = lax.psum_scatter(
        ffn_terms.astype(jnp.bfloat16), "tp", scatter_dimension=1, tiled=True
    ).astype(jnp.float32)
    ffn_squares = lax.psum(jnp.sum(ffn_sum * ffn_sum, axis=1), "tp")
    ffn_norm = ffn_sum * lax.rsqrt(ffn_squares / D + EPS)[:, None] * own_gains[2]
    return (kept_rows + 0.5 * ffn_norm).astype(jnp.bfloat16)


def solution(mesh):
    in_specs = (
        P("sp", "tp"),
        P("sp", "tp"),
        P("sp", "tp"),
        P("sp", "tp"),
        P("sp", "tp"),
        P("tp", "sp"),
        P("tp", "sp"),
        P("tp"),
        P("tp", None),
        P(None, "tp"),
        P("sp", "tp"),
        P("sp", "tp"),
        P("tp", "sp"),
    )
    out_specs = P("sp", "tp")
    return jax.shard_map(shards, mesh=mesh, in_specs=in_specs, out_specs=out_specs, check_vma=False)
```

profile of v0, /device:TPU:0, one launch (start us, length us, event | category | flops | bytes accessed | tf_op | source)
XLA Modules:
  0.0 661.8 jit_solution(8286072181642715078)
XLA Ops:
  6.5 0.7 fusion.46
  7.3 0.3 reduce_window_sum.14
  7.6 0.2 slice_reduce_fusion
  7.8 0.9 fusion.47
  8.6 0.8 multiply_bitcast_fusion
  9.4 1.1 copy.35
  10.5 1.1 copy.36
  11.6 1.5 fusion.24
  13.2 0.0 reduce-scatter.3.cloned.1.call-start
  13.3 1.2 dynamic-slice.2
  15.2 0.2 dynamic-update-slice.1
  15.4 0.2 dynamic-update-slice
  15.6 44.4 %all-reduce.2 = (f32[128]{0:T(128)S(1)}, f32[128]{0:T(128)S(1)}) all-reduce(f32[128]{0:T(128)S(1)} %dynamic-update-slice, f32[128]{0:T(128)S(1)} %dynamic-update-slice.1), channel_id=2, replica_groups=mesh['sp'=16,'tp'=2] {'sp'}, use_global_device_ids=true, to_apply=%add | all-reduce | flops 256 | bytes 2048
  60.0 0.1 reshape.87
  60.1 0.1 reshape.88
  60.2 1.1 fusion.27
  61.3 67.6 %all-gather.14.cloned.1.call-done = f32[128,128,128]{2,1,0:T(8,128)} async-done(((f32[8,128,128]{2,1,0:T(8,128)}), f32[128,128,128]{2,1,0:T(8,128)}) %all-gather.14.cloned.1.call-update) | async-done | bytes 8388624 | tf_op jit(solution)/shard_map/all_gather | solution.py:13
  128.8 20.3 %while.5 = (s32[]{:T(128)}, f32[8]{0:T(128)S(1)}, f32[8]{0:T(128)S(1)}, f32[8,128,128]{2,1,0:T(8,128)S(1)}, s32[]{:T(128)}, /*index=5*/f32[16,8]{1,0:T(8,128)S(1...) while((s32[]{:T(128)}, f32[8]{0:T(128)S(1)}, f32[8]{0:T(128)S(1)}, ...), condition=%wide.region_3.4_spmd.clone, body=%wide.region_2.3_spmd.clone.sunk | while | flops 655452 | bytes 1573449 | solution.py:25
  128.9 1.2 fusion.70
  130.2 1.2 fusion.70
  131.4 1.2 fusion.70
  132.7 1.2 fusion.70
  134.0 1.2 fusion.70
  135.2 1.2 fusion.70
  136.5 1.2 fusion.70
  137.8 1.2 fusion.70
  139.1 1.2 fusion.70
  140.3 1.2 fusion.70
  141.6 1.2 fusion.70
  142.9 1.2 fusion.70
  144.1 1.2 fusion.70
  145.4 1.2 fusion.70
  146.7 1.2 fusion.70
  148.0 1.2 fusion.70
  149.2 0.1 fusion.45
  149.3 0.1 add_maximum_fusion
  149.4 0.7 fusion.8
  150.0 0.6 multiply_reduce_fusion
  150.6 0.1 broadcast_multiply_fusion
  150.7 0.2 copy.33
  150.9 3.8 convolution_convert_fusion.1
  154.7 0.0 all-gather.8.cloned.1.call-start
  154.8 0.7 all-gather.8.cloned.1.call-update
  155.5 0.0 all-gather.10.cloned.1.call-start
  155.5 0.5 all-gather.10.cloned.1.call-update
  156.0 0.0 all-gather.12.cloned.1.call-start
  156.1 0.5 all-gather.12.cloned.1.call-update
  156.6 0.0 reduce-scatter.5.cloned.1.call-start
  156.7 4.3 reduce-scatter.3.cloned.1.call-done
  161.0 1.1 fusion.10
  162.1 2.5 psum.21
  164.5 1.2 fusion.17
  165.8 2.5 psum.22
  168.3 0.1 fusion.19
  168.4 2.2 all_gather.32
  170.6 135.7 %all-gather.8.cloned.1.call-done = bf16[2048,2816]{1,0:T(8,128)(2,1)} async-done(((bf16[128,2816]{1,0:T(8,128)(2,1)}), bf16[2048,2816]{1,0:T(8,128)(2,1)}) %all-gather.8.cloned.1.call-update) | async-done | bytes 11534352 | tf_op jit(solution)/shard_map/all_gather | solution.py:152
  306.3 5.9 fusion.57
  312.2 136.3 %all-gather.10.cloned.1.call-done = bf16[2048,2816]{1,0:T(8,128)(2,1)} async-done(((bf16[128,2816]{1,0:T(8,128)(2,1)}), bf16[2048,2816]{1,0:T(8,128)(2,1)}) %all-gather.10.cloned.1.call-update) | async-done | bytes 11534352 | tf_op jit(solution)/shard_map/all_gather | solution.py:157
  448.5 182.8 %all-gather.12.cloned.1.call-done = bf16[2816,2048]{1,0:T(8,128)(2,1)} async-done(((bf16[2816,128]{1,0:T(8,128)(2,1)}), bf16[2816,2048]{1,0:T(8,128)(2,1)}) %all-gather.12.cloned.1.call-update) | async-done | bytes 11534352 | tf_op jit(solution)/shard_map/all_gather | solution.py:162
  631.3 11.9 %convolution_convert_fusion = bf16[128,2048]{1,0:T(8,128)(2,1)} fusion(bf16[2816,2048]{1,0:T(8,128)(2,1)} %all-gather.12.cloned.1.call-done, bf16[128,2048]{1,0:T(8,128)(2,1)S(1)} %all_gather.32, bf16[2048,2816]{1,0:T(8,128)(2,1)} %all-gather.10.cloned.1.call-done, f32[128,2816]{1,0:T(8,128)S(1)} %fusion.57), kind=kOutput, calls=%fused_computation.16 | convolution fusion | flops 2955214848 | bytes 25559040 | tf_op jit(solution)/shard_map/dot_general | solution.py:161
  643.2 6.3 reduce-scatter.5.cloned.1.call-done
  649.5 1.1 fusion.14
  650.6 2.5 psum.23
  653.1 1.8 fusion.20
  (60 shorter events, 0.8 us)
Async XLA Ops:
  6.5 142.8 %copy-start = (bf16[128,1024]{1,0:T(8,128)(2,1)S(1)}, bf16[128,1024]{1,0:T(8,128)(2,1)}, u32[]{:S(2)}) copy-start(bf16[128,1024]{1,0:T(8,128)(2,1)} %param.16) | copy-start | bytes 786436
  6.5 122.3 %all-gather.14.cloned.1.call-start = ((), (), s32[]{:S(2)}) async-start(), calls=%async_computation.7 | async-start | bytes 8912896 | tf_op jit(solution)/shard_map/all_gather | solution.py:13
  13.2 147.8 %reduce-scatter.3.cloned.1.call-start = ((), (), s32[]{:S(2)}) async-start(), calls=%async_computation.2 | async-start | bytes 786432 | tf_op jit(solution)/shard_map/reduce_scatter | solution.py:138
  128.8 21.2 %copy-start.2 = (f32[8,128]{1,0:T(8,128)S(1)}, f32[8,128]{1,0:T(8,128)}, u32[]{:S(2)}) copy-start(f32[8,128]{1,0:T(8,128)} %param.20) | copy-start | bytes 12292
  149.2 1.7 copy-start.4
  149.2 1.7 copy-start.5
  150.9 5.8 copy-start.3
  150.9 13.6 %copy-start.1 = (bf16[128,1024]{1,0:T(8,128)(2,1)S(1)}, bf16[128,1024]{1,0:T(8,128)(2,1)}, u32[]{:S(2)}) copy-start(bf16[128,1024]{1,0:T(8,128)(2,1)} %param.15) | copy-start | bytes 786436
  154.7 151.6 %all-gather.8.cloned.1.call-start = ((), (), s32[]{:S(2)}) async-start(), calls=%async_computation.3 | async-start | bytes 12255232 | tf_op jit(solution)/shard_map/all_gather | solution.py:152
  155.5 293.1 %all-gather.10.cloned.1.call-start = ((), (), s32[]{:S(2)}) async-start(), calls=%async_computation.4 | async-start | bytes 12255232 | tf_op jit(solution)/shard_map/all_gather | solution.py:157
  156.0 475.3 %all-gather.12.cloned.1.call-start = ((), (), s32[]{:S(2)}) async-start(), calls=%async_computation.5 | async-start | bytes 12255232 | tf_op jit(solution)/shard_map/all_gather | solution.py:162
  156.6 492.9 %reduce-scatter.5.cloned.1.call-start = ((), (), s32[]{:S(2)}) async-start(), calls=%async_computation.6 | async-start | bytes 786432 | tf_op jit(solution)/shard_map/reduce_scatter | solution.py:164
Sparse Core Ops, SparseCore 0:
  13.3 115.4 all-gather.13
  154.8 6.0 reduce-scatter.2
  163.7 142.4 all-gather.7
  308.9 139.5 all-gather.9
  451.1 180.2 all-gather.11
  643.4 6.1 reduce-scatter.4
where the time goes:
time: 663 us; the launch traced here: 662 us
  waiting for transfers between devices  535 us (81%)
  blocking collectives  53.9 us (8%)
  other arithmetic  29.2 us (4%)
  matrix products  24.3 us (4%)
  between operations  14.3 us (2%)
    all_gather x1, waiting for transfers between devices, shards(): lax.all_gather(w_down, 'sp', axis=1, tiled=True)  183 us
    all_gather x1, waiting for transfers between devices, shards(): lax.all_gather(w_up, 'sp', axis=0, tiled=True)  136 us
    all_gather x1, waiting for transfers between devices, shards(): lax.all_gather(w_gate, 'sp', axis=0, tiled=True)  136 us
    all_gather x1, waiting for transfers between devices, carried_in(): everything = jax.tree.map(lambda part: lax.all_gather(part, axis), value)  67.6 us
    unnamed x1, blocking collectives  44.4 us
    select_n x16, other arithmetic, turn(): return jax.tree.map(lambda a, b: jnp.where(reached, a, b), new, before)  19.2 us
  transfers between devices with their start and end apart: 6, of which 6 were waited for; matrix products, arithmetic and copies ran while one was open for 2% of the time, Pallas kernels for 0%

commit v1 on v0

--- a/solution.py
+++ b/solution.py
@@ -6,6 +6,11 @@
 D = 2048
 BLOCK = 128
 EPS = 1e-06
+
+
+def swapped_in(x, axis, along):
+    sent = jnp.stack([x] * lax.axis_size(axis))
+    return jnp.concatenate(lax.all_to_all(sent, axis, 0, 0), axis=along)
 
 
 def carried_in(value, axis, combine, identity):
@@ -147,11 +152,7 @@
         jnp.bfloat16
     )
     normed_all = lax.all_gather(normed, "tp", axis=1, tiled=True)
-    gate_part = jnp.dot(
-        normed_all,
-        lax.all_gather(w_gate, "sp", axis=0, tiled=True),
-        preferred_element_type=jnp.float32,
-    )
+    gate_part = jnp.dot(normed_all, swapped_in(w_gate, "sp", 0), preferred_element_type=jnp.float32)
     up_part = jnp.dot(
         normed_all,
         lax.all_gather(w_up, "sp", axis=0, tiled=True),

time: 663 us -> 731 us (1.10)
  waiting for transfers between devices: 535 us -> 593 us
    all_to_all x0 -> x1, waiting for transfers between devices: none -> 255 us  [swapped_in(): return jnp.concatenate(lax.all_to_all(sent, axis, 0, 0), axis=along)]
    all_gather x1 -> x0, waiting for transfers between devices: 136 us -> none  [shards(): lax.all_gather(w_gate, 'sp', axis=0, tiled=True)]
    all_gather x1, waiting for transfers between devices: 136 us -> 72.3 us  [shards(): lax.all_gather(w_up, 'sp', axis=0, tiled=True)]
    all_gather x1, waiting for transfers between devices: 183 us -> 191 us  [shards(): lax.all_gather(w_down, 'sp', axis=1, tiled=True)]
  transfers between devices with their start and end apart: 6 -> 6, of which waited for: 6 -> 5; matrix products, arithmetic and copies ran while one was open for 2% -> 2% of each run, Pallas kernels for 0% -> 0%
where the time goes in v1:
time: 731 us; the launch traced here: 730 us
  waiting for transfers between devices  593 us (81%)
  blocking collectives  53.9 us (7%)
  other arithmetic  29.2 us (4%)
  matrix products  24.3 us (3%)
  between operations  14 us (2%)
  local copies, waits for them, and re-layouts  9.82 us (1%)
    all_to_all x1, waiting for transfers between devices, swapped_in(): return jnp.concatenate(lax.all_to_all(sent, axis, 0, 0), axis=along)  255 us
    all_gather x1, waiting for transfers between devices, shards(): lax.all_gather(w_down, 'sp', axis=1, tiled=True)  191 us
    all_gather x1, waiting for transfers between devices, shards(): lax.all_gather(w_up, 'sp', axis=0, tiled=True)  72.3 us
    all_gather x1, waiting for transfers between devices, carried_in(): everything = jax.tree.map(lambda part: lax.all_gather(part, axis), value)  67.6 us
    unnamed x1, blocking collectives  44.4 us
    select_n x16, other arithmetic, turn(): return jax.tree.map(lambda a, b: jnp.where(reached, a, b), new, before)  19.2 us
  transfers between devices with their start and end apart: 6, of which 5 were waited for; matrix products, arithmetic and copies ran while one was open for 2% of the time, Pallas kernels for 0%

profile of v1, /device:TPU:0, one launch (start us, length us, event | category | flops | bytes accessed | tf_op | source)
XLA Modules:
  0.0 730.0 jit_solution(12573361518333931886)
XLA Ops:
  6.5 0.0 all-gather.11.cloned.1.call-start
  6.6 0.7 fusion.46
  7.3 0.3 reduce_window_sum.14
  7.6 0.2 slice_reduce_fusion
  7.8 0.9 fusion.47
  8.7 0.8 multiply_bitcast_fusion
  9.4 1.1 copy.35
  10.6 1.1 copy.36
  11.7 1.5 fusion.24
  13.2 0.0 reduce-scatter.3.cloned.1.call-start
  13.3 1.2 dynamic-slice.2
  15.2 0.2 dynamic-update-slice.1
  15.5 0.2 dynamic-update-slice
  15.7 44.4 %all-reduce.2 = (f32[128]{0:T(128)S(1)}, f32[128]{0:T(128)S(1)}) all-reduce(f32[128]{0:T(128)S(1)} %dynamic-update-slice, f32[128]{0:T(128)S(1)} %dynamic-update-slice.1), channel_id=2, replica_groups=mesh['sp'=16,'tp'=2] {'sp'}, use_global_device_ids=true, to_apply=%add | all-reduce | flops 256 | bytes 2048
  60.1 0.1 reshape.93
  60.1 0.1 reshape.94
  60.3 1.1 fusion.27
  61.3 67.6 %all-gather.11.cloned.1.call-done = f32[128,128,128]{2,1,0:T(8,128)} async-done(((f32[8,128,128]{2,1,0:T(8,128)}), f32[128,128,128]{2,1,0:T(8,128)}) %all-gather.11.cloned.1.call-update) | async-done | bytes 8388624 | tf_op jit(solution)/shard_map/all_gather | solution.py:18
  128.9 20.3 %while.5 = (s32[]{:T(128)}, f32[8]{0:T(128)S(1)}, f32[8]{0:T(128)S(1)}, f32[8,128,128]{2,1,0:T(8,128)S(1)}, s32[]{:T(128)}, /*index=5*/f32[16,8]{1,0:T(8,128)S(1...) while((s32[]{:T(128)}, f32[8]{0:T(128)S(1)}, f32[8]{0:T(128)S(1)}, ...), condition=%wide.region_3.4_spmd.clone, body=%wide.region_2.3_spmd.clone.sunk | while | flops 655452 | bytes 1573449 | solution.py:30
  128.9 1.2 fusion.70
  130.2 1.2 fusion.70
  131.5 1.2 fusion.70
  132.7 1.2 fusion.70
  134.0 1.2 fusion.70
  135.3 1.2 fusion.70
  136.6 1.2 fusion.70
  137.8 1.2 fusion.70
  139.1 1.2 fusion.70
  140.4 1.2 fusion.70
  141.6 1.2 fusion.70
  142.9 1.2 fusion.70
  144.2 1.2 fusion.70
  145.5 1.2 fusion.70
  146.7 1.2 fusion.70
  148.0 1.2 fusion.70
  149.2 0.1 fusion.45
  149.3 0.1 add_maximum_fusion
  149.4 0.7 fusion.8
  150.1 0.6 multiply_reduce_fusion
  150.7 0.2 copy.33
  150.9 3.7 convolution_convert_fusion.1
  154.7 0.0 all-gather.7.cloned.1.call-start
  154.7 0.7 all-gather.7.cloned.1.call-update
  155.4 5.3 stack.2
  160.7 5.0 all-to-all-start
  165.8 0.0 all-gather.9.cloned.1.call-start
  165.8 0.5 all-gather.9.cloned.1.call-update
  166.4 0.0 reduce-scatter.5.cloned.1.call-start
  166.4 0.0 reduce-scatter.3.cloned.1.call-done
  166.5 1.1 fusion.10
  167.5 2.5 psum.21
  170.0 1.2 fusion.17
  171.3 2.5 psum.22
  173.7 0.1 fusion.19
  173.9 2.2 all_gather.29
  176.1 254.9 %all-to-all-done = bf16[16,128,2816]{2,1,0:T(8,128)(2,1)} async-done(((bf16[16,128,2816]{2,1,0:T(8,128)(2,1)}), bf16[16,128,2816]{2,1,0:T(8,128)(2,1)}, u32[]{:S(2)}, u32[]{:S(2)}) %all-to-all-start) | async-done | bytes 11534368 | tf_op jit(solution)/shard_map/all_to_all | solution.py:13
  430.9 6.0 fusion.57
  436.9 72.3 %all-gather.7.cloned.1.call-done = bf16[2048,2816]{1,0:T(8,128)(2,1)} async-done(((bf16[128,2816]{1,0:T(8,128)(2,1)}), bf16[2048,2816]{1,0:T(8,128)(2,1)}) %all-gather.7.cloned.1.call-update) | async-done | bytes 11534352 | tf_op jit(solution)/shard_map/all_gather | solution.py:158
  509.2 190.7 %all-gather.9.cloned.1.call-done = bf16[2816,2048]{1,0:T(8,128)(2,1)} async-done(((bf16[2816,128]{1,0:T(8,128)(2,1)}), bf16[2816,2048]{1,0:T(8,128)(2,1)}) %all-gather.9.cloned.1.call-update) | async-done | bytes 11534352 | tf_op jit(solution)/shard_map/all_gather | solution.py:163
  699.9 11.9 %convolution_convert_fusion = bf16[128,2048]{1,0:T(8,128)(2,1)} fusion(bf16[2816,2048]{1,0:T(8,128)(2,1)} %all-gather.9.cloned.1.call-done, bf16[128,2048]{1,0:T(8,128)(2,1)S(1)} %all_gather.29, bf16[2048,2816]{1,0:T(8,128)(2,1)} %all-gather.7.cloned.1.call-done, f32[128,2816]{1,0:T(8,128)S(1)} %fusion.57), kind=kOutput, calls=%fused_computation.16 | convolution fusion | flops 2955214848 | bytes 25559040 | tf_op jit(solution)/shard_map/dot_general | solution.py:162
  711.8 6.3 reduce-scatter.5.cloned.1.call-done
  718.1 1.1 fusion.14
  719.1 2.5 psum.23
  721.6 1.8 fusion.20
  (64 shorter events, 0.9 us)
Async XLA Ops:
  6.5 142.9 %copy-start = (bf16[128,1024]{1,0:T(8,128)(2,1)S(1)}, bf16[128,1024]{1,0:T(8,128)(2,1)}, u32[]{:S(2)}) copy-start(bf16[128,1024]{1,0:T(8,128)(2,1)} %param.16) | copy-start | bytes 786436
  6.5 143.5 %copy-start.4 = (f32[8,128]{1,0:T(8,128)S(1)}, f32[8,128]{1,0:T(8,128)}, u32[]{:S(2)}) copy-start(f32[8,128]{1,0:T(8,128)} %param.20) | copy-start | bytes 12292
  6.5 144.4 %copy-start.6 = (bf16[128,1024]{1,0:T(8,128)(2,1)S(1)}, bf16[128,1024]{1,0:T(8,128)(2,1)}, u32[]{:S(2)}) copy-start(bf16[128,1024]{1,0:T(8,128)(2,1)} %param.19) | copy-start | bytes 786436
  6.5 144.4 %copy-start.7 = (f32[1024]{0:T(1024)S(1)}, f32[1024]{0:T(1024)}, u32[]{:S(2)}) copy-start(f32[1024]{0:T(1024)} %param.22) | copy-start | bytes 12292
  6.5 122.3 %all-gather.11.cloned.1.call-start = ((), (), s32[]{:S(2)}) async-start(), calls=%async_computation.7 | async-start | bytes 8912896 | tf_op jit(solution)/shard_map/all_gather | solution.py:18
  13.2 153.2 %reduce-scatter.3.cloned.1.call-start = ((), (), s32[]{:S(2)}) async-start(), calls=%async_computation.3 | async-start | bytes 786432 | tf_op jit(solution)/shard_map/reduce_scatter | solution.py:143
  149.2 6.2 copy-start.2
  154.7 354.5 %all-gather.7.cloned.1.call-start = ((), (), s32[]{:S(2)}) async-start(), calls=%async_computation.4 | async-start | bytes 12255232 | tf_op jit(solution)/shard_map/all_gather | solution.py:158
  160.7 5.7 copy-start.5
  160.7 9.3 %copy-start.3 = (bf16[128,1024]{1,0:T(8,128)(2,1)S(1)}, bf16[128,1024]{1,0:T(8,128)(2,1)}, u32[]{:S(2)}) copy-start(bf16[128,1024]{1,0:T(8,128)(2,1)} %param.15) | copy-start | bytes 786436
  160.7 270.2 %all-to-all-start = ((bf16[16,128,2816]{2,1,0:T(8,128)(2,1)}), bf16[16,128,2816]{2,1,0:T(8,128)(2,1)}, u32[]{:S(2)}, u32[]{:S(2)}) async-start(bf16[16,128,2816]{2,1,0:T(8,128)(2,1)} %stack.2), calls=%async_computation.1 | async-start | bytes 23068672 | tf_op jit(solution)/shard_map/all_to_all | solution.py:13
  165.8 534.1 %all-gather.9.cloned.1.call-start = ((), (), s32[]{:S(2)}) async-start(), calls=%async_computation.5 | async-start | bytes 12255232 | tf_op jit(solution)/shard_map/all_gather | solution.py:163
  166.4 551.7 %reduce-scatter.5.cloned.1.call-start = ((), (), s32[]{:S(2)}) async-start(), calls=%async_computation.6 | async-start | bytes 786432 | tf_op jit(solution)/shard_map/reduce_scatter | solution.py:165
  430.9 292.5 %copy-start.1 = (bf16[128,1024]{1,0:T(8,128)(2,1)S(1)}, bf16[128,1024]{1,0:T(8,128)(2,1)}, u32[]{:S(2)}) copy-start(bf16[128,1024]{1,0:T(8,128)(2,1)} %param.16) | copy-start | bytes 786436
Sparse Core Ops, SparseCore 0:
  13.4 115.4 all-gather.10
  154.8 6.0 reduce-scatter.2
  163.7 345.4 all-gather.6
  511.8 188.0 all-gather.8
  711.9 6.1 reduce-scatter.4
